TPU v7x, 256 devices: a whole 4x4x8 slice. The times are simulated.
256 devices in a mesh: sp: 64 (over z, y, core), tp: 4 (over x).
Axes of the slice: x: 4, y: 4, z: 8, core: 2. Of those that a mesh axis runs over, the one named last changes fastest.
Arguments:
- residual: bfloat16 [8192, 2048], P(('sp', 'tp')), may hold values from -6 to 6
- query_content: bfloat16 [8192, 1024], P('sp', 'tp'), may hold values from -400 to 400
- query_rotary: bfloat16 [8192, 384], P('sp', 'tp'), may hold values from -16 to 16
- key_latent: bfloat16 [8192, 512], P('sp'), may hold values from -6 to 6
- rotary_key: bfloat16 [8192, 32], P('sp'), may hold values from -6 to 6
- latent_gain: float32 [512], replicated, may hold values from 0.1 to 1.9
- key_weight: bfloat16 [512, 1024], P(None, 'tp'), may hold values from -0.25 to 0.25
- value_weight: bfloat16 [512, 1024], P(None, 'tp'), may hold values from -0.25 to 0.25
- output_gain: float32 [1024], P('tp'), may hold values from 0.1 to 1.9
- output_weight: bfloat16 [1024, 2048], P('tp'), may hold values from -0.1875 to 0.1875
- mixer_gain: float32 [2048], replicated, may hold values from 0.1 to 1.9
- gate_weight: bfloat16 [2048, 5632], P('sp', 'tp'), may hold values from -0.125 to 0.125
- up_weight: bfloat16 [2048, 5632], P('sp', 'tp'), may hold values from -0.125 to 0.125
- down_weight: bfloat16 [5632, 2048], P('tp', 'sp'), may hold values from -0.078125 to 0.078125
Outputs:
- layer_out: bfloat16 [8192, 2048], P(('sp', 'tp'))
All inputs are finite; a program needn't handle non-finite values.
Results may differ from a plain program's by a relative error of at most 0.015.
Values may be sent and summed in bfloat16 or wider, within the bound.
A program may use at most 128 MiB of HBM per device.

v0:
```python
import jax
import jax.numpy as jnp
from jax import lax
from jax.sharding import PartitionSpec as P

NARROW_HEADS = 8
WIDE_HEADS = 4
NARROW_DIM = 64
WIDE_DIM = 128
ROT_DIM = 32
epsilon = 1e-06
rope_base = 500000.0


def turned_gather(arrays, axis, dims):
    turned = [jnp.moveaxis(a, dim, 0) for a, dim in zip(arrays, dims)]
    both = jnp.concatenate([t.reshape(len(t), -1) for t in turned], axis=1)
    filled, at, done = (lax.all_gather(both, axis, axis=0, tiled=True), 0, [])
    for t, dim in zip(turned, dims):
        piece = filled[:, at : at + t[0].size].reshape(-1, *t.shape[1:])
        done.append(jnp.moveaxis(piece, 0, dim))
        at += t[0].size
    return tuple(done)


def side_by_side(arrays, axis, dim, along):
    widths = [a.shape[along] for a in arrays]
    both = jnp.concatenate(arrays, axis=along)
    filled = lax.all_gather(both, axis, axis=dim, tiled=True)
    return tuple(jnp.split(filled, [sum(widths[:k]) for k in range(1, len(widths))], axis=along))


def split_up(x, dim, size):
    before, after = (x.shape[:dim], x.shape[dim + 1 :])
    return jnp.moveaxis(x.reshape(*before, size, -1, *after), dim, 0)


def summed_on_arrival(x, axis, dim):
    pieces = split_up(x, dim, lax.axis_size(axis))
    arrived = lax.all_to_all(pieces, axis, split_axis=0, concat_axis=0, tiled=True)
    return arrived.astype(jnp.float32).sum(axis=0)


def normalize(values):
    values = values.astype(jnp.float32)
    return values * lax.rsqrt(jnp.mean(values * values, axis=-1, keepdims=True) + epsilon)


def rotate(values, positions):
    half_width = values.shape[-1] // 2
    inverse = 1.0 / jnp.power(
        rope_base, jnp.arange(0, 2 * half_width, 2, dtype=jnp.float32) / (2 * half_width)
    )
    angles = positions.astype(jnp.float32)[:, None] * inverse[None, :]
    table_shape = (angles.shape[0],) + (1,) * (values.ndim - 2) + (half_width,)
    cosine_table = jnp.cos(angles).reshape(table_shape)
    sine_table = jnp.sin(angles).reshape(table_shape)
    first_half = values[..., :half_width]
    second_half = values[..., half_width:]
    return jnp.concatenate(
        [
            first_half * cosine_table - second_half * sine_table,
            second_half * cosine_table + first_half * sine_table,
        ],
        axis=-1,
    )


def group_update(carried, query_part, rotary_part, key_part, rotary_keys, value_part, factor):
    running_max, totals, accumulated = carried
    scores = (
        jnp.einsum("qhd,khd->hqk", query_part, key_part, preferred_element_type=jnp.float32)
        + jnp.einsum("qhd,kd->hqk", rotary_part, rotary_keys, preferred_element_type=jnp.float32)
    ) * factor
    new_max = jnp.max(scores, axis=-1)
    shrink = jnp.exp(running_max - new_max)
    powers = jnp.exp(scores - new_max[..., None])
    totals = totals * shrink + jnp.sum(powers, axis=-1)
    added = jnp.einsum(
        "hqk,khd->qhd", powers.astype(jnp.bfloat16), value_part, preferred_element_type=jnp.float32
    )
    accumulated = accumulated * jnp.transpose(shrink)[:, :, None] + added
    return (new_max, totals, accumulated)


def on_device(
    residual,
    query_content,
    query_rotary,
    key_latent,
    rotary_key,
    latent_gain,
    key_weight,
    value_weight,
    output_gain,
    output_weight,
    mixer_gain,
    gate_weight,
    up_weight,
    down_weight,
):
    tp_count = lax.axis_size("tp")
    narrow_dev = NARROW_HEADS // tp_count
    wide_dev = WIDE_HEADS // tp_count
    row_count = key_latent.shape[0]
    gate_whole, up_whole, down_whole = turned_gather(
        (gate_weight, up_weight, down_weight), "sp", (0, 0, 1)
    )
    positions = lax.axis_index("sp") * row_count + lax.iota(jnp.int32, row_count)
    latent = (normalize(key_latent) * latent_gain).astype(jnp.bfloat16)
    key_rows = jnp.dot(latent, key_weight, preferred_element_type=jnp.float32).astype(jnp.bfloat16)
    value_rows = jnp.dot(latent, value_weight, preferred_element_type=jnp.float32).astype(
        jnp.bfloat16
    )
    rot_keys = rotate(rotary_key.astype(jnp.float32), positions).astype(jnp.bfloat16)
    head_count = narrow_dev + wide_dev
    rot_queries = rotate(
        query_rotary.astype(jnp.float32).reshape(row_count, head_count, ROT_DIM), positions
    ).astype(jnp.bfloat16)
    narrow_cols = narrow_dev * NARROW_DIM
    query_narrow = query_content[:, :narrow_cols].reshape(row_count, narrow_dev, NARROW_DIM)
    query_wide = query_content[:, narrow_cols:].reshape(row_count, wide_dev, WIDE_DIM)
    rotary_narrow = rot_queries[:, :narrow_dev]
    rotary_wide = rot_queries[:, narrow_dev:]
    narrow_factor = (NARROW_DIM + ROT_DIM) ** (-0.5)
    wide_factor = (WIDE_DIM + ROT_DIM) ** (-0.5)

    def start_state(count, width):
        return (
            jnp.full((count, row_count), -jnp.inf, jnp.float32),
            jnp.zeros((count, row_count), jnp.float32),
            jnp.zeros((row_count, count, width), jnp.float32),
        )

    carried = (start_state(narrow_dev, NARROW_DIM), start_state(wide_dev, WIDE_DIM))
    piece_keys, piece_rotary, piece_values = side_by_side(
        (key_rows, rot_keys, value_rows), "sp", 0, 1
    )
    length = piece_keys.shape[0]
    narrow_keys = piece_keys[:, :narrow_cols].reshape(length, narrow_dev, NARROW_DIM)
    wide_keys = piece_keys[:, narrow_cols:].reshape(length, wide_dev, WIDE_DIM)
    narrow_values = piece_values[:, :narrow_cols].reshape(length, narrow_dev, NARROW_DIM)
    wide_values = piece_values[:, narrow_cols:].reshape(length, wide_dev, WIDE_DIM)
    narrow_state = group_update(
        carried[0],
        query_narrow,
        rotary_narrow,
        narrow_keys,
        piece_rotary,
        narrow_values,
        narrow_factor,
    )
    wide_state = group_update(
        carried[1], query_wide, rotary_wide, wide_keys, piece_rotary, wide_values, wide_factor
    )
    narrow_state, wide_state = (narrow_state, wide_state)

    def finish(carried):
        return normalize(carried[2] / jnp.transpose(carried[1])[:, :, None]).reshape(row_count, -1)

    mixed = (
        jnp.concatenate([finish(narrow_state), finish(wide_state)], axis=1) * output_gain
    ).astype(jnp.bfloat16)
    projected = summed_on_arrival(
        jnp.dot(mixed, output_weight, preferred_element_type=jnp.float32).astype(jnp.bfloat16),
        "tp",
        0,
    )
    middle = (residual.astype(jnp.float32) + projected).astype(jnp.bfloat16)
    normed = (normalize(middle) * mixer_gain).astype(jnp.bfloat16)
    block_normed = lax.all_gather(normed, "tp", axis=0, tiled=True)
    gate_sums = jnp.dot(block_normed, gate_whole, preferred_element_type=jnp.float32)
    up_sums = jnp.dot(block_normed, up_whole, preferred_element_type=jnp.float32)
    hidden = (jax.nn.silu(gate_sums) * up_sums).astype(jnp.bfloat16)
    channel_out = summed_on_arrival(
        jnp.dot(hidden, down_whole, preferred_element_type=jnp.float32).astype(jnp.bfloat16),
        "tp",
        0,
    )
    return (middle.astype(jnp.float32) + channel_out).astype(jnp.bfloat16)


def solution(mesh):
    placed = (
        P(("sp", "tp"), None),
        P("sp", "tp"),
        P("sp", "tp"),
        P("sp", None),
        P("sp", None),
        P(),
        P(None, "tp"),
        P(None, "tp"),
        P("tp"),
        P("tp", None),
        P(),
        P("sp", "tp"),
        P("sp", "tp"),
        P("tp", "sp"),
    )
    return jax.shard_map(
        on_device, mesh=mesh, in_specs=placed, out_specs=P(("sp", "tp"), None), check_vma=False
    )
```

profile of v0, /device:TPU:1, one launch (start us, length us, event | category | flops | bytes accessed | tf_op | source)
XLA Modules:
  0.0 234.1 jit_solution(12337247251630548791)
XLA Ops:
  6.5 0.0 copy-start
  6.5 0.0 all-gather.3.cloned.1.call-start
  6.6 0.8 convert_element_type.70
  7.3 0.1 multiply_cosine_fusion
  7.5 0.1 copy.31
  7.6 0.1 copy.32
  7.7 1.0 fusion.67
  8.8 1.3 convolution_convert_fusion.1
  10.0 1.3 convolution_convert_fusion.2
  11.3 0.8 pad_maximum_fusion.1
  12.1 0.0 all-gather.3.cloned.1.call-update
  12.1 0.0 all-gather.5.cloned.1.call-start
  12.2 1.7 pad_maximum_fusion
  13.9 0.0 all-gather.5.cloned.1.call-update
  13.9 0.7 convert.17
  14.7 0.8 slice.52
  15.4 0.1 copy.34
  15.6 86.9 %all-gather.3.cloned.1.call-done = bf16[8192,544]{1,0:T(8,128)(2,1)} async-done(((bf16[128,544]{1,0:T(8,128)(2,1)}), bf16[8192,544]{1,0:T(8,128)(2,1)}) %all-gather.3.cloned.1.call-update) | async-done | bytes 8912912 | tf_op jit(solution)/shard_map/all_gather | solution.py:29
  102.4 5.7 %fusion.90 = (bf16[8192,128]{1,0:T(8,128)(2,1)}, bf16[8192,128]{1,0:T(8,128)(2,1)}) fusion(bf16[8192,544]{1,0:T(8,128)(2,1)} %all-gather.3.cloned.1.call-done), kind=kLoop, calls=%fused_computation.99 | loop fusion | bytes 8388608 | tf_op jit(solution)/shard_map/slice | solution.py:140
  108.1 2.9 %copy.33 = bf16[8192,128]{0,1:T(8,128)(2,1)S(1)} copy(bf16[8192,128]{1,0:T(8,128)(2,1)} %get-tuple-element.7) | data formatting | bytes 4194304 | tf_op jit(solution)/shard_map/slice | solution.py:140
  111.0 4.1 %copy.36 = bf16[8192,128]{0,1:T(8,128)(2,1)} copy(bf16[8192,128]{1,0:T(8,128)(2,1)} %get-tuple-element.8) | data formatting | bytes 4194304 | tf_op jit(solution)/shard_map/slice | solution.py:142
  115.1 2.3 convolution_bitcast_fusion.2
  117.4 0.0 copy-done.3
  117.5 2.9 %fusion.91 = (f32[128]{0:T(128)S(1)}, f32[1,128,8192]{1,2,0:T(8,128)S(1)}) fusion(f32[1,128,8192]{1,2,0:T(8,128)S(1)} %convolution_bitcast_fusion.2, bf16[128,256]{1,0:T(8,128)(2,1)S(1)} %copy-done.3, bf16[8192,544]{1,0:T(8,128)(2,1)} %all-gather.3.cloned.1.call-done), kind=kOutput, calls=%fused_computation.100 | convolution fusion | flops 271581056 | bytes 10519040 | tf_op jit(solution)/shard_map/qhd,khd->hqk/dot_general | solution.py:72
  120.3 1.1 fusion.15
  121.4 3.9 %multiply_reduce_fusion = (f32[128]{0:T(128)S(1)}, f32[1,128,128]{2,1,0:T(8,128)S(1)}) fusion(f32[128]{0:T(128)S(1)} %get-tuple-element.18, f32[1,128,8192]{1,2,0:T(8,128)S(1)} %get-tuple-element.20, f32[128]{0:T(128)S(1)} %get-tuple-element.19, bf16[8192,544]{1,0:T(8,128)(2,1)} %all-gather.3.cloned.1.call-done, f32[128]{0:T(128)S(1)} %get-tuple-element.17), kind=kOutput, calls=%fused_computation.69 | convolution fusion | flops 270598016 | bytes 6359040 | tf_op jit(solution)/shard_map/hqk,khd->qhd/dot_general | solution.py:79
  125.3 2.8 %convolution_bitcast_fusion = f32[2,128,8192]{1,2,0:T(8,128)S(1)} fusion(bf16[8192,544]{1,0:T(8,128)(2,1)} %all-gather.3.cloned.1.call-done, bf16[128,3,16]{0,2,1:T(8,128)(2,1)S(1)} %get-tuple-element.9, bf16[128,3,16]{0,2,1:T(8,128)(2,1)S(1)} %get-tuple-element.10), kind=kOutput, calls=%fused_computation | convolution fusion | flops 134250496 | bytes 10510336 | tf_op jit(solution)/shard_map/qhd,kd->hqk/dot_general | solution.py:73
  128.2 2.1 fusion.92
  130.3 1.1 fusion.4
  131.5 0.5 copy-done.1
  131.9 1.6 multiply_reduce_fusion.1
  133.6 0.0 copy-start.4
  133.6 0.0 copy-done
  133.6 0.0 copy-done.5
  133.6 0.4 convolution_convert_fusion
  134.1 12.9 %all_to_all.10 = bf16[4,32,2048]{2,1,0:T(8,128)(2,1)S(1)} all-to-all(bf16[4,32,2048]{2,1,0:T(8,128)(2,1)S(1)} %bitcast.78), channel_id=1, replica_groups=mesh['sp'=64,'tp'=4] {'tp'}, dimensions={0} | all-to-all | bytes 1048576 | tf_op jit(solution)/shard_map/all_to_all | solution.py:40
  147.0 0.1 convert_reduce_fusion.1
  147.0 0.0 copy-done.2
  147.0 0.2 fusion.70
  147.2 0.0 copy-done.4
  147.2 0.1 fusion.72
  147.3 11.0 %all_gather.10 = bf16[128,2048]{1,0:T(8,128)(2,1)S(1)} all-gather(bf16[32,2048]{1,0:T(8,128)(2,1)S(1)} %fusion.72), channel_id=1, replica_groups=mesh['sp'=64,'tp'=4] {'tp'}, dimensions={0}, use_global_device_ids=true | all-gather | bytes 655360 | tf_op jit(solution)/shard_map/all_gather | solution.py:171
  158.3 44.5 %all-gather.5.cloned.1.call-done = bf16[2048,4224]{1,0:T(8,128)(2,1)} async-done(((bf16[32,4224]{1,0:T(8,128)(2,1)}), bf16[2048,4224]{1,0:T(8,128)(2,1)}) %all-gather.5.cloned.1.call-update) | async-done | bytes 17301520 | tf_op jit(solution)/shard_map/all_gather | solution.py:18
  202.8 3.6 %fusion.10 = f32[128,1408]{1,0:T(8,128)S(1)} fusion(bf16[128,2048]{1,0:T(8,128)(2,1)S(1)} %all_gather.10, bf16[2048,4224]{1,0:T(8,128)(2,1)} %all-gather.5.cloned.1.call-done), kind=kOutput, calls=%fused_computation.15 | convolution fusion | flops 738197504 | bytes 7012352 | tf_op jit(solution)/shard_map/dot_general | solution.py:172
  206.5 7.2 %fusion.20 = bf16[128,2048]{1,0:T(8,128)(2,1)S(1)} fusion(bf16[2048,4224]{1,0:T(8,128)(2,1)} %all-gather.5.cloned.1.call-done, bf16[128,2048]{1,0:T(8,128)(2,1)S(1)} %all_gather.10, f32[128,1408]{1,0:T(8,128)S(1)} %fusion.10), kind=kOutput, calls=%fused_computation.23 | convolution fusion | flops 1477738496 | bytes 13303808 | tf_op jit(solution)/shard_map/dot_general | solution.py:176
  213.7 12.8 %all_to_all.11 = bf16[4,32,2048]{2,1,0:T(8,128)(2,1)S(1)} all-to-all(bf16[4,32,2048]{2,1,0:T(8,128)(2,1)S(1)} %bitcast.79), channel_id=1, replica_groups=mesh['sp'=64,'tp'=4] {'tp'}, dimensions={0} | all-to-all | bytes 1048576 | tf_op jit(solution)/shard_map/all_to_all | solution.py:40
  226.5 0.1 convert_reduce_fusion
  226.6 0.7 fusion.73
  (16 shorter events, 0.1 us)
Async XLA Ops:
  6.5 127.1 %copy-start = (bf16[256,2048]{1,0:T(8,128)(2,1)S(1)}, bf16[256,2048]{1,0:T(8,128)(2,1)}, u32[]{:S(2)}) copy-start(bf16[256,2048]{1,0:T(8,128)(2,1)} %param.23) | copy-start | bytes 3145732
  6.5 95.9 %all-gather.3.cloned.1.call-start = ((), (), s32[]{:S(2)}) async-start(), calls=%async_computation.2 | async-start | bytes 10649600 | tf_op jit(solution)/shard_map/all_gather | solution.py:29
  12.1 190.7 %all-gather.5.cloned.1.call-start = ((), (), s32[]{:S(2)}) async-start(), calls=%async_computation.3 | async-start | bytes 17571840 | tf_op jit(solution)/shard_map/all_gather | solution.py:18
  115.1 2.3 copy-start.3
  130.3 1.6 copy-start.1
  131.9 1.7 copy-start.5
  131.9 15.1 %copy-start.2 = (bf16[32,2048]{1,0:T(8,128)(2,1)S(1)}, bf16[32,2048]{1,0:T(8,128)(2,1)}, u32[]{:S(2)}) copy-start(bf16[32,2048]{1,0:T(8,128)(2,1)} %param.14) | copy-start | bytes 393220
  133.6 13.6 %copy-start.4 = (f32[2048]{0:T(1024)S(1)}, f32[2048]{0:T(1024)}, u32[]{:S(2)}) copy-start(f32[2048]{0:T(1024)} %param.24) | copy-start | bytes 24580
Sparse Core Ops, SparseCore 0:
  12.2 90.1 all-gather.2
  105.2 97.6 all-gather.4
where the time goes:
time: 235 us; the launch traced here: 234 us
  waiting for transfers between devices  131 us (56%)
  blocking collectives  36.7 us (16%)
  matrix products  29.5 us (13%)
  local copies, waits for them, and re-layouts  14.3 us (6%)
  between operations  13.6 us (6%)
  other arithmetic  8.62 us (4%)
    all_gather x1, waiting for transfers between devices, side_by_side(): filled = lax.all_gather(both, axis, axis=dim, tiled=True)  86.9 us
    all_gather x1, waiting for transfers between devices, turned_gather(): filled, at, done = (lax.all_gather(both, axis, axis=0, tiled=True), 0, [])  44.5 us
    all_to_all x2, blocking collectives, summed_on_arrival(): lax.all_to_all(pieces, axis, split_axis=0, concat_axis=0, tiled=True)  25.7 us
    all_gather x1, blocking collectives, on_device(): block_normed = lax.all_gather(normed, 'tp', axis=0, tiled=True)  11 us
    slice x2, local copies, waits for them, and re-layouts, on_device(): piece_keys[:, :narrow_cols].reshape(length, narrow_dev, NARROW_DIM)  8.56 us
    dot_general x1, matrix products, on_device(): jnp.dot(hidden, down_whole, preferred_element_type=jnp.float32)  7.23 us
    dot_general x2, matrix products, group_update(): jnp.einsum('hqk,khd->qhd', powers.astype(jnp.bfloat16), value_part, prefe...  5.53 us
    dot_general x2, matrix products, group_update(): jnp.einsum('qhd,kd->hqk', rotary_part, rotary_keys, preferred_element_typ...  5.16 us
  transfers between devices with their start and end apart: 2, of which 2 were waited for; matrix products, arithmetic and copies ran while one was open for 15% of the time, Pallas kernels for 0%

commit v1 on v0

--- a/solution.py
+++ b/solution.py
@@ -15,7 +15,13 @@
 def turned_gather(arrays, axis, dims):
     turned = [jnp.moveaxis(a, dim, 0) for a, dim in zip(arrays, dims)]
     both = jnp.concatenate([t.reshape(len(t), -1) for t in turned], axis=1)
-    filled, at, done = (lax.all_gather(both, axis, axis=0, tiled=True), 0, [])
+    filled, at, done = (
+        jnp.concatenate(
+            lax.all_to_all(jnp.stack([both] * lax.axis_size(axis)), axis, 0, 0), axis=0
+        ),
+        0,
+        [],
+    )
     for t, dim in zip(turned, dims):
         piece = filled[:, at : at + t[0].size].reshape(-1, *t.shape[1:])
         done.append(jnp.moveaxis(piece, 0, dim))

time: 235 us -> 577 us (2.46); the launches traced: 234 us -> 569 us
  waiting for transfers between devices: 131 us -> 463 us
  blocking collectives: 36.7 us -> 21.4 us
  starting transfers between devices: 0.04 us -> 11.5 us
    all_to_all x0 -> x2, waiting for transfers between devices: none -> 374 us  [the longest x1 365 us: turned_gather(): lax.all_to_all(jnp.stack([both] * lax.axis_size(axis)), axis, 0, 0)]
    all_gather x1 -> x0, waiting for transfers between devices: 44.5 us -> none  [turned_gather(): filled, at, done = (lax.all_gather(both, axis, axis=0, tiled=True), 0, [])]
    all_to_all x2 -> x1, blocking collectives: 25.7 us -> 10.3 us  [summed_on_arrival(): lax.all_to_all(pieces, axis, split_axis=0, concat_axis=0, tiled=True)]
    all_to_all x0 -> x2, starting transfers between devices: none -> 11.5 us  [the longest x1 7.5 us: turned_gather(): lax.all_to_all(jnp.stack([both] * lax.axis_size(axis)), axis, 0, 0)]
    another operation x2 -> x3, local copies, waits for them, and re-layouts: 0.24 us -> 6.28 us  [the longest x1 6.03 us: turned_gather(): jnp.stack([both] * lax.axis_size(axis))]
  transfers between devices with their start and end apart: 2 -> 3, of which waited for: 2 -> 3; matrix products, arithmetic and copies ran while one was open for 15% -> 0% of each run, Pallas kernels for 0% -> 0%
where the time goes in v1:
time: 577 us; the launch traced here: 569 us
  waiting for transfers between devices  463 us (80%)
  matrix products  32.9 us (6%)
  blocking collectives  21.4 us (4%)
  local copies, waits for them, and re-layouts  19.6 us (3%)
  between operations  13.6 us (2%)
  starting transfers between devices  11.5 us (2%)
  other arithmetic  6.91 us (1%)
    all_to_all x1, waiting for transfers between devices, turned_gather(): lax.all_to_all(jnp.stack([both] * lax.axis_size(axis)), axis, 0, 0)  365 us
    all_gather x1, waiting for transfers between devices, side_by_side(): filled = lax.all_gather(both, axis, axis=dim, tiled=True)  88.7 us
  transfers between devices with their start and end apart: 3, of which 3 were waited for; matrix products, arithmetic and copies ran while one was open for 0% of the time, Pallas kernels for 0%

profile of v1, /device:TPU:1, one launch (start us, length us, event | category | flops | bytes accessed | tf_op | source)
XLA Modules:
  0.0 568.5 jit_solution(18373021756548918341)
XLA Ops:
  6.5 0.0 copy-start
  6.5 0.0 all-gather.2.cloned.1.call-start
  6.6 1.1 fusion.67
  7.7 0.7 convert_element_type.70
  8.4 0.1 multiply_cosine_fusion
  8.5 0.1 copy.32
  8.6 0.1 copy.31
  8.8 1.3 convolution_convert_fusion.1
  10.0 1.3 convolution_convert_fusion.2
  11.3 0.8 pad_maximum_fusion.1
  12.1 0.0 all-gather.2.cloned.1.call-update
  12.1 0.8 slice.52
  12.9 0.1 copy.34
  13.0 0.8 convert.17
  13.8 88.7 %all-gather.2.cloned.1.call-done = bf16[8192,544]{1,0:T(8,128)(2,1)} async-done(((bf16[128,544]{1,0:T(8,128)(2,1)}), bf16[8192,544]{1,0:T(8,128)(2,1)}) %all-gather.2.cloned.1.call-update) | async-done | bytes 8912912 | tf_op jit(solution)/shard_map/all_gather | solution.py:35
  102.4 2.4 convolution_bitcast_fusion.2
  104.8 0.0 copy-done.8
  104.9 0.0 slice-start.2
  104.9 3.6 fusion.91
  108.4 1.1 fusion.15
  109.6 1.7 multiply_reduce_fusion
  111.3 3.0 fusion.90
  114.3 2.9 copy.33
  117.2 2.8 convolution_bitcast_fusion
  120.0 2.1 fusion.92
  122.2 0.0 copy-start.3
  122.2 3.5 copy-done.2
  125.7 1.1 fusion.4
  126.8 2.9 copy.36
  129.8 5.6 multiply_reduce_fusion.1
  135.4 1.2 convolution_convert_fusion
  136.6 4.0 all-to-all-start
  140.6 0.0 copy-done.5
  140.6 0.0 copy-done.7
  140.7 9.0 %all-to-all-done = bf16[4,32,2048]{2,1,0:T(8,128)(2,1)S(1)} async-done(((bf16[4,32,2048]{2,1,0:T(8,128)(2,1)}), bf16[4,32,2048]{2,1,0:T(8,128)(2,1)S(1)}, u32[]{:S(2)}, u32[]{:S(2)}) %all-to-all-start) | async-done | bytes 524320 | tf_op jit(solution)/shard_map/all_to_all | solution.py:46
  149.7 6.0 %stack.2 = bf16[64,32,4224]{2,1,0:T(8,128)(2,1)} broadcast(bf16[32,4224]{1,0:T(8,128)(2,1)S(1)} %pad_maximum_fusion), dimensions={1,2} | broadcast | bytes 17571840 | tf_op jit(solution)/shard_map/stack | solution.py:20
  155.7 7.5 %all-to-all-start.1 = ((bf16[64,32,4224]{2,1,0:T(8,128)(2,1)}), bf16[64,32,4224]{2,1,0:T(8,128)(2,1)}, u32[]{:S(2)}, u32[]{:S(2)}) async-start(bf16[64,32,4224]{2,1,0:T(8,128)(2,1)} %stack.2), calls=%async_computation.1 | async-start | bytes 34603008 | tf_op jit(solution)/shard_map/all_to_all | solution.py:20
  163.2 0.1 convert_reduce_fusion.1
  163.3 0.2 fusion.70
  163.5 0.1 fusion.72
  163.6 11.1 %all_gather.7 = bf16[128,2048]{1,0:T(8,128)(2,1)S(1)} all-gather(bf16[32,2048]{1,0:T(8,128)(2,1)S(1)} %fusion.72), channel_id=1, replica_groups=mesh['sp'=64,'tp'=4] {'tp'}, dimensions={0}, use_global_device_ids=true | all-gather | bytes 655360 | tf_op jit(solution)/shard_map/all_gather | solution.py:177
  174.7 365.0 %all-to-all-done.1 = bf16[64,32,4224]{2,1,0:T(8,128)(2,1)} async-done(((bf16[64,32,4224]{2,1,0:T(8,128)(2,1)}), bf16[64,32,4224]{2,1,0:T(8,128)(2,1)}, u32[]{:S(2)}, u32[]{:S(2)}) %all-to-all-start.1) | async-done | bytes 17301536 | tf_op jit(solution)/shard_map/all_to_all | solution.py:20
  539.7 3.6 fusion.10
  543.3 0.0 copy-start.1
  543.3 7.3 %fusion.20 = bf16[128,2048]{1,0:T(8,128)(2,1)S(1)} fusion(bf16[2048,4224]{1,0:T(8,128)(2,1)} %bitcast.23, bf16[128,2048]{1,0:T(8,128)(2,1)S(1)} %all_gather.7, f32[128,1408]{1,0:T(8,128)S(1)} %fusion.10), kind=kOutput, calls=%fused_computation.23 | convolution fusion | flops 1477738496 | bytes 13303808 | tf_op jit(solution)/shard_map/dot_general | solution.py:182
  550.6 10.3 %all_to_all.15 = bf16[4,32,2048]{2,1,0:T(8,128)(2,1)S(1)} all-to-all(bf16[4,32,2048]{2,1,0:T(8,128)(2,1)S(1)} %bitcast.81), channel_id=1, replica_groups=mesh['sp'=64,'tp'=4] {'tp'}, dimensions={0} | all-to-all | bytes 1048576 | tf_op jit(solution)/shard_map/all_to_all | solution.py:46
  560.9 0.1 convert_reduce_fusion
  561.0 0.7 fusion.73
  (34 shorter events, 0.2 us)
Async XLA Ops:
  6.5 128.9 %copy-start = (bf16[256,2048]{1,0:T(8,128)(2,1)S(1)}, bf16[256,2048]{1,0:T(8,128)(2,1)}, u32[]{:S(2)}) copy-start(bf16[256,2048]{1,0:T(8,128)(2,1)} %param.23) | copy-start | bytes 3145732
  6.5 98.3 %copy-start.8 = (bf16[128,256]{1,0:T(8,128)(2,1)S(1)}, bf16[128,256]{1,0:T(8,128)(2,1)}, u32[]{:S(2)}) copy-start(bf16[128,256]{1,0:T(8,128)(2,1)} %param.15) | copy-start | bytes 196612
  6.5 95.9 %all-gather.2.cloned.1.call-start = ((), (), s32[]{:S(2)}) async-start(), calls=%async_computation.3 | async-start | bytes 10649600 | tf_op jit(solution)/shard_map/all_gather | solution.py:35
  102.4 7.1 %slice-start = ((s8[10485760]{0:T(1024)(128)(4,1)}), s8[4194304]{0:T(1024)(128)(4,1)S(1)}, s32[]{:S(2)}) async-start(s8[10485760]{0:T(1024)(128)(4,1)} %bitcast.77), calls=%async_computation.4 | async-start | bytes 8388608
  102.4 7.1 %slice-start.1 = ((s8[10485760]{0:T(1024)(128)(4,1)}), s8[4194304]{0:T(1024)(128)(4,1)S(1)}, s32[]{:S(2)}) async-start(s8[10485760]{0:T(1024)(128)(4,1)} %bitcast.77), calls=%async_computation.5 | async-start | bytes 8388608
  104.9 4.7 slice-start.2
  122.2 3.5 copy-start.2
  122.2 4.7 copy-start.3
  129.7 5.7 copy-start.10
  129.7 10.9 %copy-start.5 = (bf16[1408,32]{0,1:T(8,128)(2,1)S(1)}, bf16[1408,32]{0,1:T(8,128)(2,1)}, u32[]{:S(2)}) copy-start(bf16[1408,32]{0,1:T(8,128)(2,1)} %param.27) | copy-start | bytes 270340
  129.8 10.9 %copy-start.6 = (bf16[32,1408]{1,0:T(8,128)(2,1)S(1)}, bf16[32,1408]{1,0:T(8,128)(2,1)}, u32[]{:S(2)}) copy-start(bf16[32,1408]{1,0:T(8,128)(2,1)} %param.26) | copy-start | bytes 270340
  129.8 10.9 %copy-start.7 = (bf16[32,1408]{1,0:T(8,128)(2,1)S(1)}, bf16[32,1408]{1,0:T(8,128)(2,1)}, u32[]{:S(2)}) copy-start(bf16[32,1408]{1,0:T(8,128)(2,1)} %param.25) | copy-start | bytes 270340
  136.6 13.0 %all-to-all-start = ((bf16[4,32,2048]{2,1,0:T(8,128)(2,1)}), bf16[4,32,2048]{2,1,0:T(8,128)(2,1)S(1)}, u32[]{:S(2)}, u32[]{:S(2)}) async-start(bf16[4,32,2048]{2,1,0:T(8,128)(2,1)} %bitcast.21), calls=%async_computation | async-start | bytes 1048576 | tf_op jit(solution)/shard_map/all_to_all | solution.py:46
  155.7 7.6 %copy-start.4 = (bf16[32,2048]{1,0:T(8,128)(2,1)S(1)}, bf16[32,2048]{1,0:T(8,128)(2,1)}, u32[]{:S(2)}) copy-start(bf16[32,2048]{1,0:T(8,128)(2,1)} %param.14) | copy-start | bytes 393220
  155.7 7.8 %copy-start.9 = (f32[2048]{0:T(1024)S(1)}, f32[2048]{0:T(1024)}, u32[]{:S(2)}) copy-start(f32[2048]{0:T(1024)} %param.24) | copy-start | bytes 24580
  155.7 384.0 %all-to-all-start.1 = ((bf16[64,32,4224]{2,1,0:T(8,128)(2,1)}), bf16[64,32,4224]{2,1,0:T(8,128)(2,1)}, u32[]{:S(2)}, u32[]{:S(2)}) async-start(bf16[64,32,4224]{2,1,0:T(8,128)(2,1)} %stack.2), calls=%async_computation.1 | async-start | bytes 34603008 | tf_op jit(solution)/shard_map/all_to_all | solution.py:20
  543.3 18.4 %copy-start.1 = (bf16[256,2048]{1,0:T(8,128)(2,1)S(1)}, bf16[256,2048]{1,0:T(8,128)(2,1)}, u32[]{:S(2)}) copy-start(bf16[256,2048]{1,0:T(8,128)(2,1)} %param.23) | copy-start | bytes 3145732
Sparse Core Ops, SparseCore 0:
  12.2 90.1 all-gather.1
